TPU v7x, 32 devices: a whole 2x2x4 slice. The times are simulated.
32 devices in a mesh: fs: 8 (over z, y), tp: 4 (over x, core).
Axes of the slice: x: 2, y: 2, z: 4, core: 2. Of those that a mesh axis runs over, the one named last changes fastest.
Arguments:
- tokens: bfloat16 [3072, 2048], P(('fs', 'tp')), may hold values from -6 to 6
- ffn1_gain: float32 [2048], replicated, may hold values from 0.1 to 1.9
- ffn1_gate: bfloat16 [2048, 5632], P('fs', 'tp'), may hold values from -0.125 to 0.125
- ffn1_up: bfloat16 [2048, 5632], P('fs', 'tp'), may hold values from -0.125 to 0.125
- ffn1_down: bfloat16 [5632, 2048], P('tp', 'fs'), may hold values from -0.078125 to 0.078125
- mix_gain: float32 [2048], replicated, may hold values from 0.1 to 1.9
- lru_in_weight: bfloat16 [2048, 1536], P('fs', 'tp'), may hold values from -0.125 to 0.125
- lru_gate_weight: bfloat16 [2048, 1536], P('fs', 'tp'), may hold values from -0.125 to 0.125
- conv_weight: bfloat16 [4, 1536], P(None, 'tp'), may hold values from -3 to 3
- gate_a_weight: bfloat16 [24, 64, 64], P('tp'), may hold values from -0.75 to 0.75
- gate_x_weight: bfloat16 [24, 64, 64], P('tp'), may hold values from -0.75 to 0.75
- decay_param: float32 [1536], P('tp'), may hold values from 3.7 to 9
- mix_out_weight: bfloat16 [1536, 2048], P('tp', 'fs'), may hold values from -0.15625 to 0.15625
- ffn2_gain: float32 [2048], replicated, may hold values from 0.1 to 1.9
- ffn2_gate: bfloat16 [2048, 5632], P('fs', 'tp'), may hold values from -0.125 to 0.125
- ffn2_up: bfloat16 [2048, 5632], P('fs', 'tp'), may hold values from -0.125 to 0.125
- ffn2_down: bfloat16 [5632, 2048], P('tp', 'fs'), may hold values from -0.078125 to 0.078125
Outputs:
- layer_out: bfloat16 [3072, 2048], P(('fs', 'tp'))
All inputs are finite; a program needn't handle non-finite values.
Results may differ from a plain program's by a relative error of at most 0.017.
Values may be sent and summed in bfloat16 or wider, within the bound.
A program may use at most 64 MiB of HBM per device.

v0:
```python
import jax
import jax.numpy as jnp
from jax import lax
from jax.sharding import PartitionSpec as P

EPS = 1e-06


def rms_rows(values, gain):
    wide = values.astype(jnp.float32)
    scale = lax.rsqrt(jnp.mean(wide * wide, axis=-1, keepdims=True) + EPS)
    return (wide * scale * gain).astype(jnp.bfloat16)


def gather_rows(values):
    return lax.all_gather(values, "tp", axis=0, tiled=True)


def pair_step(rows, pieces):
    return (
        jnp.dot(rows, pieces[0], preferred_element_type=jnp.float32),
        jnp.dot(rows, pieces[1], preferred_element_type=jnp.float32),
    )


def block_hidden(rows, gate_weight, up_weight):
    gate, upper = pair_step(
        rows,
        (
            lax.all_gather(gate_weight, "fs", axis=0, tiled=True),
            lax.all_gather(up_weight, "fs", axis=0, tiled=True),
        ),
    )
    return (jax.nn.silu(gate) * upper).astype(jnp.bfloat16)


def block_terms(hidden, down_weight):
    return jnp.dot(
        hidden,
        lax.all_gather(down_weight, "fs", axis=1, tiled=True),
        preferred_element_type=jnp.float32,
    )


def reduce_rows(terms):
    return lax.psum_scatter(
        terms.astype(jnp.bfloat16), "tp", scatter_dimension=0, tiled=True
    ).astype(jnp.float32)


def whole_sum(terms):
    return lax.psum(terms.astype(jnp.bfloat16), "tp").astype(jnp.float32)


def combine(earlier, later):
    return (earlier[0] * later[0], later[0] * earlier[1] + later[1])


def mixer_terms(
    rows,
    lru_in_weight,
    lru_gate_weight,
    conv_weight,
    gate_a_weight,
    gate_x_weight,
    decay_param,
    mix_out_weight,
):
    lru_x, lru_gate = pair_step(
        rows,
        (
            lax.all_gather(lru_in_weight, "fs", axis=0, tiled=True),
            lax.all_gather(lru_gate_weight, "fs", axis=0, tiled=True),
        ),
    )
    lru_low = lru_x.astype(jnp.bfloat16).astype(jnp.float32)
    gate_low = lru_gate.astype(jnp.bfloat16).astype(jnp.float32)
    length = rows.shape[0]
    taps_count = conv_weight.shape[0]
    padded = jnp.pad(lru_low, ((taps_count - 1, 0), (0, 0)))
    taps = conv_weight.astype(jnp.float32)
    conv = jnp.zeros_like(lru_low)
    for offset in range(taps_count):
        conv = (
            conv + taps[offset] * padded[taps_count - 1 - offset : taps_count - 1 - offset + length]
        )
    conv_low = conv.astype(jnp.bfloat16)
    blocks = conv_low.reshape(length, gate_a_weight.shape[0], gate_a_weight.shape[1])
    recall = jax.nn.sigmoid(
        jnp.einsum(
            "sbi,bij->sbj", blocks, gate_a_weight, preferred_element_type=jnp.float32
        ).reshape(length, -1)
    )
    admit = jax.nn.sigmoid(
        jnp.einsum(
            "sbi,bij->sbj", blocks, gate_x_weight, preferred_element_type=jnp.float32
        ).reshape(length, -1)
    )
    log_keep = -8.0 * recall * jax.nn.softplus(-decay_param)
    drive = jnp.sqrt(-jnp.expm1(2.0 * log_keep)) * admit * conv_low.astype(jnp.float32)
    _, state = lax.associative_scan(combine, (jnp.exp(log_keep), drive), axis=0)
    mixed = (state * jax.nn.gelu(gate_low)).astype(jnp.bfloat16)
    return jnp.dot(
        mixed,
        lax.all_gather(mix_out_weight, "fs", axis=1, tiled=True),
        preferred_element_type=jnp.float32,
    )


def body(
    tokens,
    ffn1_gain,
    ffn1_gate,
    ffn1_up,
    ffn1_down,
    mix_gain,
    lru_in_weight,
    lru_gate_weight,
    conv_weight,
    gate_a_weight,
    gate_x_weight,
    decay_param,
    mix_out_weight,
    ffn2_gain,
    ffn2_gate,
    ffn2_up,
    ffn2_down,
):
    local = tokens.shape[0]
    whole = gather_rows(tokens)
    terms = block_terms(block_hidden(rms_rows(whole, ffn1_gain), ffn1_gate, ffn1_up), ffn1_down)
    first = (whole.astype(jnp.float32) + 0.5 * whole_sum(terms)).astype(jnp.bfloat16)
    terms = mixer_terms(
        rms_rows(first, mix_gain),
        lru_in_weight,
        lru_gate_weight,
        conv_weight,
        gate_a_weight,
        gate_x_weight,
        decay_param,
        mix_out_weight,
    )
    second_all = (first.astype(jnp.float32) + whole_sum(terms)).astype(jnp.bfloat16)
    rows = rms_rows(second_all, ffn2_gain)
    second = lax.dynamic_slice_in_dim(second_all, lax.axis_index("tp") * local, local, 0)
    terms = block_terms(block_hidden(rows, ffn2_gate, ffn2_up), ffn2_down)
    return (second.astype(jnp.float32) + 0.5 * reduce_rows(terms)).astype(jnp.bfloat16)


def solution(mesh):
    in_specs = (
        P(("fs", "tp"), None),
        P(),
        P("fs", "tp"),
        P("fs", "tp"),
        P("tp", "fs"),
        P(),
        P("fs", "tp"),
        P("fs", "tp"),
        P(None, "tp"),
        P("tp", None, None),
        P("tp", None, None),
        P("tp"),
        P("tp", "fs"),
        P(),
        P("fs", "tp"),
        P("fs", "tp"),
        P("tp", "fs"),
    )
    out_specs = P(("fs", "tp"), None)
    return jax.shard_map(body, mesh=mesh, in_specs=in_specs, out_specs=out_specs, check_vma=False)
```

profile of v0, /device:TPU:0, one launch (start us, length us, event | category | flops | bytes accessed | tf_op | source)
XLA Modules:
  0.0 873.1 jit_solution(14798320163815893249)
XLA Ops:
  9.4 21.9 %all-gather.11.cloned.1.call-done = bf16[384,2048]{1,0:T(8,128)(2,1)} async-done(((bf16[96,2048]{1,0:T(8,128)(2,1)}), bf16[384,2048]{1,0:T(8,128)(2,1)}) %all-gather.11.cloned.1.call-update) | async-done | bytes 1572880 | tf_op jit(solution)/shard_map/all_gather | solution.py:16
  31.3 1.8 fusion.3
  33.1 92.7 %all-gather.13.cloned.1.call-done = bf16[2048,1408]{1,0:T(8,128)(2,1)} async-done(((bf16[256,1408]{1,0:T(8,128)(2,1)}), bf16[2048,1408]{1,0:T(8,128)(2,1)}) %all-gather.13.cloned.1.call-update) | async-done | bytes 5767184 | tf_op jit(solution)/shard_map/all_gather | solution.py:30
  125.8 7.1 fusion.33
  132.9 85.6 %all-gather.15.cloned.1.call-done = bf16[2048,1408]{1,0:T(8,128)(2,1)} async-done(((bf16[256,1408]{1,0:T(8,128)(2,1)}), bf16[2048,1408]{1,0:T(8,128)(2,1)}) %all-gather.15.cloned.1.call-update) | async-done | bytes 5767184 | tf_op jit(solution)/shard_map/all_gather | solution.py:31
  218.5 93.2 %all-gather.17.cloned.1.call-done = bf16[1408,2048]{1,0:T(8,128)(2,1)} async-done(((bf16[1408,256]{1,0:T(8,128)(2,1)}), bf16[1408,2048]{1,0:T(8,128)(2,1)}) %all-gather.17.cloned.1.call-update) | async-done | bytes 5767184 | tf_op jit(solution)/shard_map/all_gather | solution.py:40
  311.8 11.3 %convolution_convert_fusion.2 = bf16[384,2048]{1,0:T(8,128)(2,1)} fusion(bf16[1408,2048]{1,0:T(8,128)(2,1)} %all-gather.17.cloned.1.call-done, bf16[2048,1408]{1,0:T(8,128)(2,1)} %all-gather.15.cloned.1.call-done, f32[384,1408]{1,0:T(8,128)} %fusion.33, bf16[384,2048]{1,0:T(8,128)(2,1)S(1)} %copy-done.2, f32[2048]{0:T(1024)S(1)} %copy-done.16, ...), kind=kOutput, calls=%fused_computation.25 | convolution fusion | flops 4436361216 | bytes 16852480 | tf_op jit(solution)/shard_map/dot_general | solution.py:38
  325.5 38.8 %all-reduce.20.cloned.1.call-done = bf16[384,2048]{1,0:T(8,128)(2,1)} async-done(((bf16[384,2048]{1,0:T(8,128)(2,1)}), bf16[384,2048]{1,0:T(8,128)(2,1)}) %all-reduce.20.cloned.1.call-update) | async-done | bytes 1572880 | tf_op jit(solution)/shard_map/psum | solution.py:52
  364.3 2.3 fusion.7
  366.5 44.0 %all-gather.19.cloned.1.call-done = bf16[2048,384]{1,0:T(8,128)(2,1)} async-done(((bf16[256,384]{1,0:T(8,128)(2,1)}), bf16[2048,384]{1,0:T(8,128)(2,1)}) %all-gather.19.cloned.1.call-update) | async-done | bytes 1572880 | tf_op jit(solution)/shard_map/all_gather | solution.py:72
  410.6 2.4 fusion.20
  416.4 1.9 multiply_exponential_fusion
  428.0 1.9 fusion.65
  482.3 17.9 %all-gather.23.cloned.1.call-done = bf16[384,2048]{1,0:T(8,128)(2,1)} async-done(((bf16[384,256]{1,0:T(8,128)(2,1)}), bf16[384,2048]{1,0:T(8,128)(2,1)}) %all-gather.23.cloned.1.call-update) | async-done | bytes 1572880 | tf_op jit(solution)/shard_map/all_gather | solution.py:105
  500.2 5.3 convolution_convert_fusion.1
  507.7 39.0 %all-reduce.22.cloned.1.call-done = bf16[384,2048]{1,0:T(8,128)(2,1)} async-done(((bf16[384,2048]{1,0:T(8,128)(2,1)}), bf16[384,2048]{1,0:T(8,128)(2,1)}) %all-reduce.22.cloned.1.call-update) | async-done | bytes 1572880 | tf_op jit(solution)/shard_map/psum | solution.py:52
  546.7 2.1 fusion
  548.8 92.3 %all-gather.25.cloned.1.call-done = bf16[2048,1408]{1,0:T(8,128)(2,1)} async-done(((bf16[256,1408]{1,0:T(8,128)(2,1)}), bf16[2048,1408]{1,0:T(8,128)(2,1)}) %all-gather.25.cloned.1.call-update) | async-done | bytes 5767184 | tf_op jit(solution)/shard_map/all_gather | solution.py:30
  641.1 6.6 fusion.37
  647.7 86.1 %all-gather.27.cloned.1.call-done = bf16[2048,1408]{1,0:T(8,128)(2,1)} async-done(((bf16[256,1408]{1,0:T(8,128)(2,1)}), bf16[2048,1408]{1,0:T(8,128)(2,1)}) %all-gather.27.cloned.1.call-update) | async-done | bytes 5767184 | tf_op jit(solution)/shard_map/all_gather | solution.py:31
  733.8 93.2 %all-gather.29.cloned.1.call-done = bf16[1408,2048]{1,0:T(8,128)(2,1)} async-done(((bf16[1408,256]{1,0:T(8,128)(2,1)}), bf16[1408,2048]{1,0:T(8,128)(2,1)}) %all-gather.29.cloned.1.call-update) | async-done | bytes 5767184 | tf_op jit(solution)/shard_map/all_gather | solution.py:40
  827.1 11.3 %convolution_convert_fusion = bf16[384,2048]{1,0:T(8,128)(2,1)} fusion(bf16[1408,2048]{1,0:T(8,128)(2,1)} %all-gather.29.cloned.1.call-done, bf16[2048,1408]{1,0:T(8,128)(2,1)} %all-gather.27.cloned.1.call-done, f32[384,1408]{1,0:T(8,128)} %fusion.37, bf16[384,2048]{1,0:T(8,128)(2,1)S(1)} %get-tuple-element.10, f32[2048]{0:T(1024)S(1)} %copy-done.19, ...), kind=kOutput, calls=%fused_computation.23 | convolution fusion | flops 4436361216 | bytes 16852480 | tf_op jit(solution)/shard_map/dot_general | solution.py:38
  838.4 26.3 %reduce-scatter.2.cloned.1.call-done = bf16[96,2048]{1,0:T(8,128)(2,1)} async-done(((bf16[384,2048]{1,0:T(8,128)(2,1)}), bf16[96,2048]{1,0:T(8,128)(2,1)}) %reduce-scatter.2.cloned.1.call-update) | async-done | bytes 393232 | tf_op jit(solution)/shard_map/reduce_scatter | solution.py:46
  864.7 1.9 add_convert_fusion
  (172 shorter events, 72.4 us)
Async XLA Ops:
  6.5 407.0 %copy-start = (bf16[6,64,64]{2,1,0:T(8,128)(2,1)S(1)}, bf16[6,64,64]{2,1,0:T(8,128)(2,1)}, u32[]{:S(2)}) copy-start(bf16[6,64,64]{2,1,0:T(8,128)(2,1)} %param.26) | copy-start | bytes 147460
  6.5 119.3 %copy-start.16 = (f32[2048]{0:T(1024)S(1)}, f32[2048]{0:T(1024)}, u32[]{:S(2)}) copy-start(f32[2048]{0:T(1024)} %param.18) | copy-start | bytes 24580
  6.5 24.7 %all-gather.11.cloned.1.call-start = ((), (), s32[]{:S(2)}) async-start(), calls=%async_computation.1 | async-start | bytes 1966080 | tf_op jit(solution)/shard_map/all_gather | solution.py:16
  7.3 118.5 %all-gather.13.cloned.1.call-start = ((), (), s32[]{:S(2)}) async-start(), calls=%async_computation.2 | async-start | bytes 6488064 | tf_op jit(solution)/shard_map/all_gather | solution.py:30
  8.0 210.5 %all-gather.15.cloned.1.call-start = ((), (), s32[]{:S(2)}) async-start(), calls=%async_computation.3 | async-start | bytes 6488064 | tf_op jit(solution)/shard_map/all_gather | solution.py:31
  8.7 303.0 %all-gather.17.cloned.1.call-start = ((), (), s32[]{:S(2)}) async-start(), calls=%async_computation.4 | async-start | bytes 6488064 | tf_op jit(solution)/shard_map/all_gather | solution.py:40
  9.3 354.9 %all-reduce.20.cloned.1.call-start = ((), (), s32[]{:S(2)}) async-start(), calls=%async_computation.5 | async-start | bytes 3145728 | tf_op jit(solution)/shard_map/psum | solution.py:52
  33.1 278.7 %copy-start.2 = (bf16[384,2048]{1,0:T(8,128)(2,1)S(1)}, bf16[384,2048]{1,0:T(8,128)(2,1)}, u32[]{:S(2)}) copy-start(bf16[384,2048]{1,0:T(8,128)(2,1)} %all-gather.11.cloned.1.call-done) | copy-start | bytes 4718596
  323.1 87.5 %all-gather.19.cloned.1.call-start = ((), (), s32[]{:S(2)}) async-start(), calls=%async_computation.6 | async-start | bytes 1769472 | tf_op jit(solution)/shard_map/all_gather | solution.py:72
  323.6 158.6 %all-gather.21.cloned.1.call-start = ((), (), s32[]{:S(2)}) async-start(), calls=%async_computation.7 | async-start | bytes 1769472 | tf_op jit(solution)/shard_map/all_gather | solution.py:73
  324.4 175.8 %all-gather.23.cloned.1.call-start = ((), (), s32[]{:S(2)}) async-start(), calls=%async_computation.8 | async-start | bytes 1769472 | tf_op jit(solution)/shard_map/all_gather | solution.py:105
  325.1 221.5 %all-reduce.22.cloned.1.call-start = ((), (), s32[]{:S(2)}) async-start(), calls=%async_computation.9 | async-start | bytes 3145728 | tf_op jit(solution)/shard_map/psum | solution.py:52
  325.5 85.1 %copy-start.17 = (f32[2048]{0:T(1024)S(1)}, f32[2048]{0:T(1024)}, u32[]{:S(2)}) copy-start(f32[2048]{0:T(1024)} %param.22) | copy-start | bytes 24580
  366.5 46.5 %copy-start.13 = (f32[384]{0:T(512)}, f32[384]{0:T(512)S(1)}, u32[]{:S(2)}) copy-start(f32[384]{0:T(512)S(1)} %add_rsqrt_fusion.1) | copy-start | bytes 4612
  462.7 12.0 %copy-start.5 = (f32[5,384]{1,0:T(8,128)S(1)}, f32[5,384]{1,0:T(8,128)}, u32[]{:S(2)}) copy-start(f32[5,384]{1,0:T(8,128)} %slice.249) | copy-start | bytes 23044
  462.7 12.1 %copy-start.6 = (f32[5,384]{1,0:T(8,128)S(1)}, f32[5,384]{1,0:T(8,128)}, u32[]{:S(2)}) copy-start(f32[5,384]{1,0:T(8,128)} %slice.268) | copy-start | bytes 23044
  480.3 19.9 %copy-start.14 = (f32[384]{0:T(512)S(1)}, f32[384]{0:T(512)}, u32[]{:S(2)}) copy-start(f32[384]{0:T(512)} %copy-done.13) | copy-start | bytes 4612
  480.3 19.9 %copy-start.18 = (f32[2048]{0:T(1024)S(1)}, f32[2048]{0:T(1024)}, u32[]{:S(2)}) copy-start(f32[2048]{0:T(1024)} %param.22) | copy-start | bytes 24580
  505.5 135.6 %all-gather.25.cloned.1.call-start = ((), (), s32[]{:S(2)}) async-start(), calls=%async_computation.10 | async-start | bytes 6488064 | tf_op jit(solution)/shard_map/all_gather | solution.py:30
  506.1 227.8 %all-gather.27.cloned.1.call-start = ((), (), s32[]{:S(2)}) async-start(), calls=%async_computation.11 | async-start | bytes 6488064 | tf_op jit(solution)/shard_map/all_gather | solution.py:31
  506.8 320.3 %all-gather.29.cloned.1.call-start = ((), (), s32[]{:S(2)}) async-start(), calls=%async_computation.12 | async-start | bytes 6488064 | tf_op jit(solution)/shard_map/all_gather | solution.py:40
  507.4 133.7 %copy-start.19 = (f32[2048]{0:T(1024)S(1)}, f32[2048]{0:T(1024)}, u32[]{:S(2)}) copy-start(f32[2048]{0:T(1024)} %param.30) | copy-start | bytes 24580
  507.4 357.3 %reduce-scatter.2.cloned.1.call-start = ((), (), s32[]{:S(2)}) async-start(), calls=%async_computation.13 | async-start | bytes 1966080 | tf_op jit(solution)/shard_map/reduce_scatter | solution.py:46
  827.1 39.5 %copy-start.1 = (bf16[6,64,64]{2,1,0:T(8,128)(2,1)S(1)}, bf16[6,64,64]{2,1,0:T(8,128)(2,1)}, u32[]{:S(2)}) copy-start(bf16[6,64,64]{2,1,0:T(8,128)(2,1)} %param.26) | copy-start | bytes 147460
  (9 other events, 46.1 us)
Sparse Core Ops, SparseCore 0:
  8.9 22.3 all-gather.10
  33.5 92.3 all-gather.12
  128.0 90.4 all-gather.14
  220.4 91.2 all-gather.16
  323.2 41.0 all-reduce.19
  366.3 44.2 all-gather.18
  412.8 42.5 all-gather.20
  457.4 42.7 all-gather.22
  505.6 41.0 all-reduce.21
  548.7 92.3 all-gather.24
  643.3 90.4 all-gather.26
  735.7 91.2 all-gather.28
  838.5 26.1 reduce-scatter.1
where the time goes:
time: 875 us; the launch traced here: 873 us
  waiting for transfers between devices  737 us (84%)
  local copies, waits for them, and re-layouts  51.5 us (6%)
  matrix products  44.7 us (5%)
  other arithmetic  24.8 us (3%)
  between operations  13.8 us (2%)
    all_gather x2, waiting for transfers between devices, block_terms(): lax.all_gather(down_weight, 'fs', axis=1, tiled=True)  186 us
    all_gather x2, waiting for transfers between devices, block_hidden(): lax.all_gather(gate_weight, 'fs', axis=0, tiled=True)  185 us
    all_gather x2, waiting for transfers between devices, block_hidden(): lax.all_gather(up_weight, 'fs', axis=0, tiled=True)  172 us
    psum x2, waiting for transfers between devices, whole_sum(): return lax.psum(terms.astype(jnp.bfloat16), 'tp').astype(jnp.float32)  77.8 us
    slice x49, local copies, waits for them, and re-layouts, mixer_terms(): _, state = lax.associative_scan(combine, (jnp.exp(log_keep), drive), axis=0)  47 us
    all_gather x1, waiting for transfers between devices, mixer_terms(): lax.all_gather(lru_in_weight, 'fs', axis=0, tiled=True)  44 us
    reduce_scatter x1, waiting for transfers between devices, reduce_rows(): lax.psum_scatter(terms.astype(jnp.bfloat16), 'tp', scatter_dimension=0, t...  26.3 us
    dot_general x2, matrix products, block_terms(): jnp.dot(hidden, lax.all_gather(down_weight, 'fs', axis=1, tiled=True), pr...  22.6 us
  transfers between devices with their start and end apart: 13, of which 12 were waited for; matrix products, arithmetic and copies ran while one was open for 10% of the time, Pallas kernels for 0%

commit v1 on v0

--- a/solution.py
+++ b/solution.py
@@ -1,9 +1,18 @@
+import functools
 import jax
 import jax.numpy as jnp
 from jax import lax
 from jax.sharding import PartitionSpec as P
 
 EPS = 1e-06
+
+
+def set_the_core(tile_in, comm_axis):
+    after = lax.all_gather(tile_in, axis_name=comm_axis).sum(axis=0)
+    return after
+
+
+spread_sector_all = functools.partial(set_the_core, comm_axis="tp")
 
 
 def rms_rows(values, gain):
@@ -49,7 +58,7 @@
 
 
 def whole_sum(terms):
-    return lax.psum(terms.astype(jnp.bfloat16), "tp").astype(jnp.float32)
+    return spread_sector_all(terms.astype(jnp.bfloat16)).astype(jnp.float32)
 
 
 def combine(earlier, later):

time: 875 us -> 882 us (level)
  other arithmetic: 24.8 us -> 34.6 us
    all_gather x0 -> x2, waiting for transfers between devices: none -> 84.8 us  [set_the_core(): after = lax.all_gather(tile_in, axis_name=comm_axis).sum(axis=0)]
    psum x2 -> x0, waiting for transfers between devices: 77.8 us -> none  [whole_sum(): return lax.psum(terms.astype(jnp.bfloat16), 'tp').astype(jnp.float32)]
    reduce_sum x0 -> x2, other arithmetic: none -> 9.94 us  [set_the_core(): after = lax.all_gather(tile_in, axis_name=comm_axis).sum(axis=0)]
  transfers between devices with their start and end apart: 13 -> 13, of which waited for: 12 -> 12; matrix products, arithmetic and copies ran while one was open for 10% -> 12% of each run, Pallas kernels for 0% -> 0%
where the time goes in v1:
time: 882 us; the launch traced here: 880 us
  waiting for transfers between devices  734 us (83%)
  local copies, waits for them, and re-layouts  51.6 us (6%)
  matrix products  45.4 us (5%)
  other arithmetic  34.6 us (4%)
  between operations  13.8 us (2%)
    all_gather x2, waiting for transfers between devices, block_terms(): lax.all_gather(down_weight, 'fs', axis=1, tiled=True)  186 us
    all_gather x2, waiting for transfers between devices, block_hidden(): lax.all_gather(gate_weight, 'fs', axis=0, tiled=True)  181 us
    all_gather x2, waiting for transfers between devices, block_hidden(): lax.all_gather(up_weight, 'fs', axis=0, tiled=True)  171 us
    all_gather x2, waiting for transfers between devices, set_the_core(): after = lax.all_gather(tile_in, axis_name=comm_axis).sum(axis=0)  84.8 us
    slice x49, local copies, waits for them, and re-layouts, mixer_terms(): _, state = lax.associative_scan(combine, (jnp.exp(log_keep), drive), axis=0)  47 us
    all_gather x1, waiting for transfers between devices, mixer_terms(): lax.all_gather(lru_in_weight, 'fs', axis=0, tiled=True)  38.2 us
    reduce_scatter x1, waiting for transfers between devices, reduce_rows(): lax.psum_scatter(terms.astype(jnp.bfloat16), 'tp', scatter_dimension=0, t...  26.3 us
    dot_general x2, matrix products, block_terms(): jnp.dot(hidden, lax.all_gather(down_weight, 'fs', axis=1, tiled=True), pr...  22.5 us
  transfers between devices with their start and end apart: 13, of which 12 were waited for; matrix products, arithmetic and copies ran while one was open for 12% of the time, Pallas kernels for 0%

profile of v1, /device:TPU:0, one launch (start us, length us, event | category | flops | bytes accessed | tf_op | source)
XLA Modules:
  0.0 880.1 jit_solution(17935002308620244880)
XLA Ops:
  9.4 21.9 %all-gather.15.cloned.1.call-done = bf16[384,2048]{1,0:T(8,128)(2,1)} async-done(((bf16[96,2048]{1,0:T(8,128)(2,1)}), bf16[384,2048]{1,0:T(8,128)(2,1)}) %all-gather.15.cloned.1.call-update) | async-done | bytes 1572880 | tf_op jit(solution)/shard_map/all_gather | solution.py:25
  33.1 92.7 %all-gather.17.cloned.1.call-done = bf16[2048,1408]{1,0:T(8,128)(2,1)} async-done(((bf16[256,1408]{1,0:T(8,128)(2,1)}), bf16[2048,1408]{1,0:T(8,128)(2,1)}) %all-gather.17.cloned.1.call-update) | async-done | bytes 5767184 | tf_op jit(solution)/shard_map/all_gather | solution.py:39
  125.8 7.1 fusion.33
  132.9 85.6 %all-gather.19.cloned.1.call-done = bf16[2048,1408]{1,0:T(8,128)(2,1)} async-done(((bf16[256,1408]{1,0:T(8,128)(2,1)}), bf16[2048,1408]{1,0:T(8,128)(2,1)}) %all-gather.19.cloned.1.call-update) | async-done | bytes 5767184 | tf_op jit(solution)/shard_map/all_gather | solution.py:40
  218.5 93.2 %all-gather.21.cloned.1.call-done = bf16[1408,2048]{1,0:T(8,128)(2,1)} async-done(((bf16[1408,256]{1,0:T(8,128)(2,1)}), bf16[1408,2048]{1,0:T(8,128)(2,1)}) %all-gather.21.cloned.1.call-update) | async-done | bytes 5767184 | tf_op jit(solution)/shard_map/all_gather | solution.py:49
  311.8 11.3 %convolution_convert_fusion.2 = bf16[384,2048]{1,0:T(8,128)(2,1)} fusion(bf16[1408,2048]{1,0:T(8,128)(2,1)} %all-gather.21.cloned.1.call-done, bf16[2048,1408]{1,0:T(8,128)(2,1)} %all-gather.19.cloned.1.call-done, f32[384,1408]{1,0:T(8,128)} %fusion.33, bf16[384,2048]{1,0:T(8,128)(2,1)S(1)} %copy-done.2, f32[2048]{0:T(1024)S(1)} %copy-done.17, ...), kind=kOutput, calls=%fused_computation.25 | convolution fusion | flops 4436361216 | bytes 16852480 | tf_op jit(solution)/shard_map/dot_general | solution.py:47
  325.5 42.3 %all-gather.35.cloned.1.call-done = bf16[1536,2048]{1,0:T(8,128)(2,1)} async-done(((bf16[384,2048]{1,0:T(8,128)(2,1)}), bf16[1536,2048]{1,0:T(8,128)(2,1)}) %all-gather.35.cloned.1.call-update) | async-done | bytes 6291472 | tf_op jit(solution)/shard_map/all_gather | solution.py:11
  367.8 5.7 reduce_sum.52
  373.5 2.3 fusion.7
  375.8 38.2 %all-gather.23.cloned.1.call-done = bf16[2048,384]{1,0:T(8,128)(2,1)} async-done(((bf16[256,384]{1,0:T(8,128)(2,1)}), bf16[2048,384]{1,0:T(8,128)(2,1)}) %all-gather.23.cloned.1.call-update) | async-done | bytes 1572880 | tf_op jit(solution)/shard_map/all_gather | solution.py:81
  414.0 2.4 fusion.20
  419.9 1.9 multiply_exponential_fusion
  431.5 1.9 fusion.65
  485.9 17.8 %all-gather.27.cloned.1.call-done = bf16[384,2048]{1,0:T(8,128)(2,1)} async-done(((bf16[384,256]{1,0:T(8,128)(2,1)}), bf16[384,2048]{1,0:T(8,128)(2,1)}) %all-gather.27.cloned.1.call-update) | async-done | bytes 1572880 | tf_op jit(solution)/shard_map/all_gather | solution.py:114
  503.7 5.3 convolution_convert_fusion.1
  511.2 42.5 %all-gather.37.cloned.1.call-done = bf16[1536,2048]{1,0:T(8,128)(2,1)} async-done(((bf16[384,2048]{1,0:T(8,128)(2,1)}), bf16[1536,2048]{1,0:T(8,128)(2,1)}) %all-gather.37.cloned.1.call-update) | async-done | bytes 6291472 | tf_op jit(solution)/shard_map/all_gather | solution.py:11
  553.8 4.2 reduce_sum.54
  558.0 1.9 fusion
  559.9 88.3 %all-gather.29.cloned.1.call-done = bf16[2048,1408]{1,0:T(8,128)(2,1)} async-done(((bf16[256,1408]{1,0:T(8,128)(2,1)}), bf16[2048,1408]{1,0:T(8,128)(2,1)}) %all-gather.29.cloned.1.call-update) | async-done | bytes 5767184 | tf_op jit(solution)/shard_map/all_gather | solution.py:39
  648.1 7.2 fusion.37
  655.4 85.5 %all-gather.31.cloned.1.call-done = bf16[2048,1408]{1,0:T(8,128)(2,1)} async-done(((bf16[256,1408]{1,0:T(8,128)(2,1)}), bf16[2048,1408]{1,0:T(8,128)(2,1)}) %all-gather.31.cloned.1.call-update) | async-done | bytes 5767184 | tf_op jit(solution)/shard_map/all_gather | solution.py:40
  740.9 93.2 %all-gather.33.cloned.1.call-done = bf16[1408,2048]{1,0:T(8,128)(2,1)} async-done(((bf16[1408,256]{1,0:T(8,128)(2,1)}), bf16[1408,2048]{1,0:T(8,128)(2,1)}) %all-gather.33.cloned.1.call-update) | async-done | bytes 5767184 | tf_op jit(solution)/shard_map/all_gather | solution.py:49
  834.1 11.2 %convolution_convert_fusion = bf16[384,2048]{1,0:T(8,128)(2,1)} fusion(bf16[1408,2048]{1,0:T(8,128)(2,1)} %all-gather.33.cloned.1.call-done, bf16[2048,1408]{1,0:T(8,128)(2,1)} %all-gather.31.cloned.1.call-done, f32[384,1408]{1,0:T(8,128)} %fusion.37, bf16[384,2048]{1,0:T(8,128)(2,1)S(1)} %copy-done.3, f32[2048]{0:T(1024)S(1)} %copy-done.20, ...), kind=kOutput, calls=%fused_computation.23 | convolution fusion | flops 4436361216 | bytes 16852480 | tf_op jit(solution)/shard_map/dot_general | solution.py:47
  845.4 26.3 %reduce-scatter.2.cloned.1.call-done = bf16[96,2048]{1,0:T(8,128)(2,1)} async-done(((bf16[384,2048]{1,0:T(8,128)(2,1)}), bf16[96,2048]{1,0:T(8,128)(2,1)}) %reduce-scatter.2.cloned.1.call-update) | async-done | bytes 393232 | tf_op jit(solution)/shard_map/reduce_scatter | solution.py:55
  (176 shorter events, 76.2 us)
Async XLA Ops:
  6.5 410.5 %copy-start = (bf16[6,64,64]{2,1,0:T(8,128)(2,1)S(1)}, bf16[6,64,64]{2,1,0:T(8,128)(2,1)}, u32[]{:S(2)}) copy-start(bf16[6,64,64]{2,1,0:T(8,128)(2,1)} %param.26) | copy-start | bytes 147460
  6.5 119.3 %copy-start.17 = (f32[2048]{0:T(1024)S(1)}, f32[2048]{0:T(1024)}, u32[]{:S(2)}) copy-start(f32[2048]{0:T(1024)} %param.18) | copy-start | bytes 24580
  6.5 24.7 %all-gather.15.cloned.1.call-start = ((), (), s32[]{:S(2)}) async-start(), calls=%async_computation.1 | async-start | bytes 1966080 | tf_op jit(solution)/shard_map/all_gather | solution.py:25
  7.3 118.5 %all-gather.17.cloned.1.call-start = ((), (), s32[]{:S(2)}) async-start(), calls=%async_computation.2 | async-start | bytes 6488064 | tf_op jit(solution)/shard_map/all_gather | solution.py:39
  8.0 210.5 %all-gather.19.cloned.1.call-start = ((), (), s32[]{:S(2)}) async-start(), calls=%async_computation.3 | async-start | bytes 6488064 | tf_op jit(solution)/shard_map/all_gather | solution.py:40
  8.7 303.0 %all-gather.21.cloned.1.call-start = ((), (), s32[]{:S(2)}) async-start(), calls=%async_computation.4 | async-start | bytes 6488064 | tf_op jit(solution)/shard_map/all_gather | solution.py:49
  9.3 358.5 %all-gather.35.cloned.1.call-start = ((), (), s32[]{:S(2)}) async-start(), calls=%async_computation.12 | async-start | bytes 7864320 | tf_op jit(solution)/shard_map/all_gather | solution.py:11
  33.1 278.7 %copy-start.2 = (bf16[384,2048]{1,0:T(8,128)(2,1)S(1)}, bf16[384,2048]{1,0:T(8,128)(2,1)}, u32[]{:S(2)}) copy-start(bf16[384,2048]{1,0:T(8,128)(2,1)} %all-gather.15.cloned.1.call-done) | copy-start | bytes 4718596
  323.1 90.9 %all-gather.23.cloned.1.call-start = ((), (), s32[]{:S(2)}) async-start(), calls=%async_computation.5 | async-start | bytes 1769472 | tf_op jit(solution)/shard_map/all_gather | solution.py:81
  323.7 162.3 %all-gather.25.cloned.1.call-start = ((), (), s32[]{:S(2)}) async-start(), calls=%async_computation.6 | async-start | bytes 1769472 | tf_op jit(solution)/shard_map/all_gather | solution.py:82
  324.4 179.3 %all-gather.27.cloned.1.call-start = ((), (), s32[]{:S(2)}) async-start(), calls=%async_computation.7 | async-start | bytes 1769472 | tf_op jit(solution)/shard_map/all_gather | solution.py:114
  325.2 228.6 %all-gather.37.cloned.1.call-start = ((), (), s32[]{:S(2)}) async-start(), calls=%async_computation.13 | async-start | bytes 7864320 | tf_op jit(solution)/shard_map/all_gather | solution.py:11
  373.5 40.5 %copy-start.18 = (f32[2048]{0:T(1024)S(1)}, f32[2048]{0:T(1024)}, u32[]{:S(2)}) copy-start(f32[2048]{0:T(1024)} %param.22) | copy-start | bytes 24580
  375.8 40.7 %copy-start.14 = (f32[384]{0:T(512)}, f32[384]{0:T(512)S(1)}, u32[]{:S(2)}) copy-start(f32[384]{0:T(512)S(1)} %add_rsqrt_fusion.1) | copy-start | bytes 4612
  466.2 12.1 %copy-start.7 = (f32[5,384]{1,0:T(8,128)S(1)}, f32[5,384]{1,0:T(8,128)}, u32[]{:S(2)}) copy-start(f32[5,384]{1,0:T(8,128)} %slice.268) | copy-start | bytes 23044
  483.9 19.8 %copy-start.15 = (f32[384]{0:T(512)S(1)}, f32[384]{0:T(512)}, u32[]{:S(2)}) copy-start(f32[384]{0:T(512)} %copy-done.14) | copy-start | bytes 4612
  483.9 19.8 %copy-start.19 = (f32[2048]{0:T(1024)S(1)}, f32[2048]{0:T(1024)}, u32[]{:S(2)}) copy-start(f32[2048]{0:T(1024)} %param.22) | copy-start | bytes 24580
  509.1 139.1 %all-gather.29.cloned.1.call-start = ((), (), s32[]{:S(2)}) async-start(), calls=%async_computation.8 | async-start | bytes 6488064 | tf_op jit(solution)/shard_map/all_gather | solution.py:39
  509.7 231.2 %all-gather.31.cloned.1.call-start = ((), (), s32[]{:S(2)}) async-start(), calls=%async_computation.9 | async-start | bytes 6488064 | tf_op jit(solution)/shard_map/all_gather | solution.py:40
  510.4 323.7 %all-gather.33.cloned.1.call-start = ((), (), s32[]{:S(2)}) async-start(), calls=%async_computation.10 | async-start | bytes 6488064 | tf_op jit(solution)/shard_map/all_gather | solution.py:49
  511.0 360.7 %reduce-scatter.2.cloned.1.call-start = ((), (), s32[]{:S(2)}) async-start(), calls=%async_computation.11 | async-start | bytes 1966080 | tf_op jit(solution)/shard_map/reduce_scatter | solution.py:55
  558.0 90.2 %copy-start.20 = (f32[2048]{0:T(1024)S(1)}, f32[2048]{0:T(1024)}, u32[]{:S(2)}) copy-start(f32[2048]{0:T(1024)} %param.30) | copy-start | bytes 24580
  648.1 186.0 %copy-start.3 = (bf16[384,2048]{1,0:T(8,128)(2,1)S(1)}, bf16[384,2048]{1,0:T(8,128)(2,1)}, u32[]{:S(2)}) copy-start(bf16[384,2048]{1,0:T(8,128)(2,1)} %get-tuple-element.10) | copy-start | bytes 4718596
  834.1 39.5 %copy-start.1 = (bf16[6,64,64]{2,1,0:T(8,128)(2,1)S(1)}, bf16[6,64,64]{2,1,0:T(8,128)(2,1)}, u32[]{:S(2)}) copy-start(bf16[6,64,64]{2,1,0:T(8,128)(2,1)} %param.26) | copy-start | bytes 147460
  (10 other events, 58.3 us)
Sparse Core Ops, SparseCore 0:
  8.9 22.3 all-gather.14
  33.5 92.3 all-gather.16
  128.0 90.4 all-gather.18
  220.4 91.2 all-gather.20
  323.2 44.5 all-gather.34
  369.8 44.1 all-gather.22
  416.2 42.5 all-gather.24
  460.9 42.7 all-gather.26
  509.2 44.5 all-gather.36
  555.8 92.3 all-gather.28
  650.3 90.4 all-gather.30
  742.8 91.2 all-gather.32
  845.5 26.1 reduce-scatter.1
